TPU v7x, 256 devices: a whole 4x4x8 slice. The times are simulated.
256 devices in a mesh: sp: 64 (over z, x, core), tp: 4 (over y).
Axes of the slice: x: 4, y: 4, z: 8, core: 2. Of those that a mesh axis runs over, the one named last changes fastest.
Arguments:
- query_one: bfloat16 [16384, 512], P('sp', 'tp'), may hold values from -100 to 100, as said below
- key_one: bfloat16 [16384, 512], P('sp', 'tp'), may hold values from -8 to 8
- query_two: bfloat16 [16384, 512], P('sp', 'tp'), may hold values from -100 to 100, as said below
- key_two: bfloat16 [16384, 512], P('sp', 'tp'), may hold values from -8 to 8
- values: bfloat16 [16384, 1024], P('sp', 'tp'), may hold values from -6 to 6
- mix_lambda: float32 [8], P('tp'), may hold values from 0.3 to 0.8
- head_gain: float32 [128], replicated, may hold values from 0.1 to 1.9
- residual_in: bfloat16 [16384, 2048], P(('sp', 'tp')), may hold values from -6 to 6
- out_weight: bfloat16 [1024, 2048], replicated, may hold values from -0.1875 to 0.1875
- norm_gain: float32 [2048], replicated, may hold values from 0.1 to 1.9
- route_ids: int32 [16384, 2], P(('sp', 'tp')), may hold values from 0 to 127, all different within a row; in each aligned block of 64 rows (0 to 63, 64 to 127, ...) at most 2 rows name the same one
- route_logits: float32 [16384, 2], P(('sp', 'tp')), may hold values from -6 to 6
- group_prob: float32 [16384], P(('sp', 'tp')), may hold values from 0.25 to 1
- gate_weight: bfloat16 [128, 2048, 1024], P('sp', None, 'tp'), may hold values from -0.125 to 0.125
- up_weight: bfloat16 [128, 2048, 1024], P('sp', None, 'tp'), may hold values from -0.125 to 0.125
- down_weight: bfloat16 [128, 1024, 2048], P('sp', 'tp'), may hold values from -0.1875 to 0.1875
Outputs:
- layer_out: bfloat16 [16384, 2048], P(('sp', 'tp'))
Inputs may be any that keep to these rules, and one draw needn't show every extreme that they name: `query_one`: drawn together with key_one. `query_two`: drawn together with key_two. `route_ids`: the experts of a row differ. In the rows of one device no expert is named more than 2 times, a bound that some block reaches.
All inputs are finite; a program needn't handle non-finite values.
Results may differ from a plain program's by a relative error of at most 0.014.
Values may be sent and summed in bfloat16 or wider, within the bound.
A program may use at most 128 MiB of HBM per device.

v0:
```python
import math

import jax
import jax.numpy as jnp
from jax import lax
from jax.sharding import PartitionSpec as P

norm_epsilon = 1e-06


def sent_together(arrays, axis, dim, along):
    widths = [a.shape[along] for a in arrays]
    both = jnp.concatenate(arrays, axis=along)
    whole = lax.all_gather(both, axis, axis=dim, tiled=True)
    return tuple(jnp.split(whole, [sum(widths[:k]) for k in range(1, len(widths))], axis=along))


def on_device(
    query_one,
    key_one,
    query_two,
    key_two,
    values,
    mix_lambda,
    head_gain,
    residual_in,
    out_weight,
    norm_gain,
    route_ids,
    route_logits,
    group_prob,
    gate_weight,
    up_weight,
    down_weight,
):
    row_count = query_one.shape[0]
    head_count = mix_lambda.shape[0]
    qk_dim = query_one.shape[1] // head_count
    v_dim = values.shape[1] // head_count
    score_scale = 1.0 / math.sqrt(qk_dim)
    query_a = query_one.reshape(row_count, head_count, qk_dim)
    query_b = query_two.reshape(row_count, head_count, qk_dim)

    def absorb(state, queries, keys, vals):
        running_max, running_sum, accumulated = state
        scores = (
            jnp.einsum("thd,shd->hts", queries, keys, preferred_element_type=jnp.float32)
            * score_scale
        )
        new_max = jnp.maximum(running_max, jnp.max(scores, axis=-1))
        shrink = jnp.exp(running_max - new_max)
        expo = jnp.exp(scores - new_max[..., None])
        running_sum = running_sum * shrink + jnp.sum(expo, axis=-1)
        accumulated = accumulated * shrink[..., None] + jnp.einsum(
            "hts,shd->htd", expo.astype(jnp.bfloat16), vals, preferred_element_type=jnp.float32
        )
        return (new_max, running_sum, accumulated)

    start_state = (
        jnp.full((head_count, row_count), -1e30, jnp.float32),
        jnp.zeros((head_count, row_count), jnp.float32),
        jnp.zeros((head_count, row_count, v_dim), jnp.float32),
    )
    folded = (start_state, start_state)
    key_a, key_b, vals = sent_together((key_one, key_two, values), "sp", 0, 1)
    length = key_a.shape[0]
    key_span = 2048
    block_count = length // key_span
    blocks = (
        key_a.reshape(block_count, key_span, head_count, qk_dim),
        key_b.reshape(block_count, key_span, head_count, qk_dim),
        vals.reshape(block_count, key_span, head_count, v_dim),
    )

    def advance(state, key_block):
        first_state, second_state = state
        block_a, block_b, block_v = key_block
        return (
            (
                absorb(first_state, query_a, block_a, block_v),
                absorb(second_state, query_b, block_b, block_v),
            ),
            None,
        )

    folded, _ = lax.scan(advance, folded, blocks)
    first_state, second_state = folded
    read_a = first_state[2] / first_state[1][..., None]
    read_b = second_state[2] / second_state[1][..., None]
    combined = read_a - mix_lambda[:, None, None] * read_b
    combined = (
        combined
        * lax.rsqrt(jnp.mean(combined * combined, axis=-1, keepdims=True) + norm_epsilon)
        * head_gain
    )
    attended = (
        combined.astype(jnp.bfloat16).transpose(1, 0, 2).reshape(row_count, head_count * v_dim)
    )
    share = row_count // lax.axis_size("tp")
    token_heads = lax.all_to_all(attended, "tp", split_axis=0, concat_axis=1, tiled=True)
    mix = jnp.dot(token_heads, out_weight, preferred_element_type=jnp.float32)
    hidden_f = (residual_in.astype(jnp.float32) + mix).astype(jnp.bfloat16).astype(jnp.float32)
    normed = (
        hidden_f
        * lax.rsqrt(jnp.mean(hidden_f * hidden_f, axis=-1, keepdims=True) + norm_epsilon)
        * norm_gain
    ).astype(jnp.bfloat16)
    width = normed.shape[1]
    top_count = route_ids.shape[1]
    local_experts = gate_weight.shape[0]
    expert_count = local_experts * lax.axis_size("sp")
    capacity = max(2, 2 * share * top_count // expert_count)
    flat_ids = route_ids.reshape(-1)
    one_hot = (flat_ids[:, None] == jnp.arange(expert_count, dtype=jnp.int32)[None, :]).astype(
        jnp.int32
    )
    earlier = jnp.cumsum(one_hot, axis=0) - one_hot
    rank = jnp.sum(earlier * one_hot, axis=1)
    slot_of = flat_ids * capacity + rank
    table = (
        jnp.arange(expert_count * capacity, dtype=jnp.int32)[:, None] == slot_of[None, :]
    ).astype(jnp.bfloat16)
    outgoing = jnp.dot(
        table, jnp.repeat(normed, top_count, axis=0), preferred_element_type=jnp.float32
    )
    outgoing = outgoing.astype(jnp.bfloat16).reshape(expert_count, capacity, width)
    arrived = lax.all_to_all(outgoing, "sp", split_axis=0, concat_axis=0, tiled=True)
    slot_count = arrived.shape[1]
    grouped = arrived.reshape(-1, local_experts, slot_count, width)
    everyone = lax.all_gather(grouped, "tp", axis=0, tiled=True)
    gate = jnp.einsum("sexd,edf->sexf", everyone, gate_weight, preferred_element_type=jnp.float32)
    upper = jnp.einsum("sexd,edf->sexf", everyone, up_weight, preferred_element_type=jnp.float32)
    middle = (jax.nn.silu(gate) * upper).astype(jnp.bfloat16)
    part_sum = jnp.einsum("sexf,efd->sexd", middle, down_weight, preferred_element_type=jnp.float32)
    summed = lax.psum_scatter(part_sum.astype(jnp.bfloat16), "tp", scatter_dimension=0, tiled=True)
    answered = summed.reshape(-1, slot_count, width)
    returned = lax.all_to_all(answered, "sp", split_axis=0, concat_axis=0, tiled=True)
    picked = returned.reshape(expert_count * capacity, width)[slot_of].astype(jnp.float32)
    picked = picked.reshape(share, top_count, width)
    route_weight = jax.nn.softmax(route_logits, axis=-1) * group_prob[:, None]
    moe = jnp.sum(picked * route_weight[..., None], axis=1)
    return (hidden_f + moe).astype(jnp.bfloat16)


def solution(mesh):
    in_specs = (
        P("sp", "tp"),
        P("sp", "tp"),
        P("sp", "tp"),
        P("sp", "tp"),
        P("sp", "tp"),
        P("tp"),
        P(),
        P(("sp", "tp"), None),
        P(),
        P(),
        P(("sp", "tp"), None),
        P(("sp", "tp"), None),
        P(("sp", "tp")),
        P("sp", None, "tp"),
        P("sp", None, "tp"),
        P("sp", "tp", None),
    )
    out_specs = P(("sp", "tp"), None)
    return jax.shard_map(
        on_device, mesh=mesh, in_specs=in_specs, out_specs=out_specs, check_vma=False
    )
```

profile of v0, /device:TPU:1, one launch (start us, length us, event | category | flops | bytes accessed | tf_op | source)
XLA Modules:
  0.0 503.8 jit_solution(2592242817500888282)
XLA Ops:
  6.5 1.8 pad_maximum_fusion
  11.7 101.9 %all-gather.3.cloned.1.call-done = bf16[16384,512]{1,0:T(8,128)(2,1)} async-done(((bf16[256,512]{1,0:T(8,128)(2,1)}), bf16[16384,512]{1,0:T(8,128)(2,1)}) %all-gather.3.cloned.1.call-update) | async-done | bytes 16777232 | tf_op jit(solution)/shard_map/all_gather | solution.py:14
  113.5 5.7 %fusion.62 = (bf16[16384,128]{1,0:T(8,128)(2,1)}, bf16[16384,128]{1,0:T(8,128)(2,1)}) fusion(bf16[16384,512]{1,0:T(8,128)(2,1)} %all-gather.3.cloned.1.call-done), kind=kLoop, calls=%fused_computation.84 | loop fusion | bytes 16777216 | tf_op jit(solution)/shard_map/split | solution.py:15
  119.3 14.7 %reshape.131 = bf16[8,2048,2,64]{3,2,1,0:T(2,128)(2,1)} reshape(bf16[16384,128]{1,0:T(8,128)(2,1)} %get-tuple-element.162) | data formatting | bytes 8388608 | tf_op jit(solution)/shard_map/reshape | solution.py:70
  134.0 20.2 %copy.31 = bf16[8,2048,2,64]{1,3,2,0:T(8,128)(2,1)} copy(bf16[8,2048,2,64]{3,2,1,0:T(2,128)(2,1)} %reshape.131) | data formatting | bytes 8388608
  154.2 14.7 %reshape.133 = bf16[8,2048,2,64]{3,2,1,0:T(2,128)(2,1)} reshape(bf16[16384,128]{1,0:T(8,128)(2,1)} %get-tuple-element.161) | data formatting | bytes 8388608 | tf_op jit(solution)/shard_map/reshape | solution.py:71
  168.9 20.2 %copy.33 = bf16[8,2048,2,64]{1,3,2,0:T(8,128)(2,1)} copy(bf16[8,2048,2,64]{3,2,1,0:T(2,128)(2,1)} %reshape.133) | data formatting | bytes 8388608
  189.1 7.1 %split.13 = bf16[16384,256]{1,0:T(8,128)(2,1)} slice(bf16[16384,512]{1,0:T(8,128)(2,1)} %all-gather.3.cloned.1.call-done), slice={[0:16384], [256:512]} | slice | bytes 16777216 | tf_op jit(solution)/shard_map/split | solution.py:15
  196.1 12.5 %reshape.132 = bf16[8,2048,2,128]{3,2,1,0:T(2,128)(2,1)} reshape(bf16[16384,256]{1,0:T(8,128)(2,1)} %split.13) | data formatting | bytes 16777216 | tf_op jit(solution)/shard_map/reshape | solution.py:72
  208.7 74.9 %while.21 = (s32[]{:T(128)}, f32[2,256]{1,0:T(2,128)S(1)}, f32[2,256]{1,0:T(2,128)S(1)}, f32[2,256,128]{2,1,0:T(8,128)S(1)}, f32[2,256]{1,0:T(2,128)S(1)}, /*ind...) while((s32[]{:T(128)}, f32[2,256]{1,0:T(2,128)S(1)}, ...), condition=%wide.region_5.6_spmd.clone, body=%wide.region_0.5_spmd.clone.sunk | while | flops 822481920 | bytes 31655060 | solution.py:86
  208.7 1.9 bitcast_reduce_fusion.4
  211.3 1.8 bitcast_reduce_fusion.5
  213.8 1.8 constant_dynamic-slice_fusion.2
  215.7 1.2 fusion.91
  216.9 1.2 fusion.90
  218.1 1.8 bitcast_reduce_fusion.4
  220.6 1.8 bitcast_reduce_fusion.5
  223.2 1.8 constant_dynamic-slice_fusion.2
  225.0 1.2 fusion.91
  227.5 1.8 bitcast_reduce_fusion.4
  230.0 1.8 bitcast_reduce_fusion.5
  232.5 1.8 constant_dynamic-slice_fusion.2
  234.4 1.2 fusion.91
  235.6 1.2 fusion.90
  236.8 1.8 bitcast_reduce_fusion.4
  239.3 1.8 bitcast_reduce_fusion.5
  241.9 1.8 constant_dynamic-slice_fusion.2
  243.7 1.2 fusion.91
  246.2 1.8 bitcast_reduce_fusion.4
  248.7 1.8 bitcast_reduce_fusion.5
  251.2 1.8 constant_dynamic-slice_fusion.2
  253.1 1.2 fusion.91
  254.3 1.2 fusion.90
  255.5 1.8 bitcast_reduce_fusion.4
  258.0 1.8 bitcast_reduce_fusion.5
  260.6 1.8 constant_dynamic-slice_fusion.2
  262.4 1.2 fusion.91
  264.9 1.8 bitcast_reduce_fusion.4
  267.4 1.8 bitcast_reduce_fusion.5
  270.0 1.8 constant_dynamic-slice_fusion.2
  271.8 1.2 fusion.91
  274.2 1.8 bitcast_reduce_fusion.4
  276.7 1.8 bitcast_reduce_fusion.5
  279.3 1.8 constant_dynamic-slice_fusion.2
  281.1 1.2 fusion.91
  285.0 4.0 all-to-all-start
  289.0 4.8 all-to-all-done
  293.8 3.2 multiply_reduce_fusion.1
  299.3 1.5 convolution_convert_fusion
  300.8 1.5 reshape.115
  302.3 35.5 %all_to_all.29 = bf16[128,2,2048]{2,1,0:T(2,128)(2,1)S(1)} all-to-all(bf16[128,2,2048]{2,1,0:T(2,128)(2,1)} %reshape.115), channel_id=1, replica_groups=mesh['sp'=64,'tp'=4] {'sp'}, dimensions={0} | all-to-all | bytes 2097152 | tf_op jit(solution)/shard_map/all_to_all | solution.py:127
  337.8 1.6 copy.37
  339.4 45.8 %all-gather.5.cloned.1.call-done = bf16[256,2,2,2048]{3,0,2,1:T(8,128)(2,1)} async-done(((bf16[64,2,2,2048]{3,0,2,1:T(8,128)(2,1)}), bf16[256,2,2,2048]{3,0,2,1:T(8,128)(2,1)}) %all-gather.5.cloned.1.call-update) | async-done | bytes 4194320 | tf_op jit(solution)/shard_map/all_gather | solution.py:130
  385.2 4.1 fusion.41
  389.3 7.3 %convert_bitcast_fusion = bf16[256,2,2,2048]{3,0,2,1:T(8,128)(2,1)} fusion(bf16[2,256,2048]{2,1,0:T(8,128)(2,1)S(1)} %copy-done, bf16[256,2,2,2048]{3,0,2,1:T(8,128)(2,1)} %all-gather.5.cloned.1.call-done, bf16[2,2048,256]{2,1,0:T(8,128)(2,1)} %param.32, f32[256,2,2,256]{3,0,2,1:T(8,128)S(1)} %fusion.41), kind=kOutput, calls=%fused_computation.43 | convolution fusion | flops 2151153664 | bytes 13631488 | tf_op jit(solution)/shard_map/sexf,efd->sexd/dot_general | solution.py:134
  396.7 50.0 %reduce-scatter.2.cloned.1.call-done = bf16[64,2,2,2048]{3,0,2,1:T(8,128)(2,1)} async-done(((bf16[256,2,2,2048]{3,0,2,1:T(8,128)(2,1)}), bf16[64,2,2,2048]{3,0,2,1:T(8,128)(2,1)}) %reduce-scatter.2.cloned.1.call-update) | async-done | bytes 1048592 | tf_op jit(solution)/shard_map/reduce_scatter | solution.py:135
  446.7 3.4 copy.38
  450.1 10.9 %all-to-all-start.2 = ((bf16[128,2,2048]{2,1,0:T(2,128)(2,1)}), bf16[128,2,2048]{2,1,0:T(2,128)(2,1)}, u32[]{:S(2)}, u32[]{:S(2)}) async-start(bf16[128,2,2048]{2,1,0:T(2,128)(2,1)} %bitcast.14), calls=%async_computation.3 | async-start | bytes 2097152 | tf_op jit(solution)/shard_map/all_to_all | solution.py:137
  461.4 27.6 %all-to-all-done.2 = bf16[128,2,2048]{2,1,0:T(2,128)(2,1)} async-done(((bf16[128,2,2048]{2,1,0:T(2,128)(2,1)}), bf16[128,2,2048]{2,1,0:T(2,128)(2,1)}, u32[]{:S(2)}, u32[]{:S(2)}) %all-to-all-start.2) | async-done | bytes 1048608 | tf_op jit(solution)/shard_map/all_to_all | solution.py:137
  489.0 1.5 reshape.118
  490.5 1.7 gather_fusion
  492.2 1.7 reshape.119
  493.9 1.5 multiply_reduce_fusion
  495.5 1.8 add_convert_fusion
  (118 shorter events, 24.9 us)
Async XLA Ops:
  6.5 382.8 %copy-start = (bf16[2,256,2048]{2,1,0:T(8,128)(2,1)S(1)}, bf16[2,256,2048]{2,1,0:T(8,128)(2,1)}, u32[]{:S(2)}) copy-start(bf16[2,256,2048]{2,1,0:T(8,128)(2,1)} %param.33) | copy-start | bytes 6291460
  6.5 107.0 %all-gather.3.cloned.1.call-start = ((), (), s32[]{:S(2)}) async-start(), calls=%async_computation.4 | async-start | bytes 17039360 | tf_op jit(solution)/shard_map/all_gather | solution.py:14
  208.7 74.9 %copy-start.8 = (f32[2]{0:T(128)S(1)}, f32[2]{0:T(128)}, u32[]{:S(2)}) copy-start(f32[2]{0:T(128)} %param.23) | copy-start | bytes 28
  208.7 75.2 %copy-start.6 = (f32[128]{0:T(128)S(1)}, f32[128]{0:T(128)}, u32[]{:S(2)}) copy-start(f32[128]{0:T(128)} %param.24) | copy-start | bytes 1540
  208.7 85.1 %copy-start.2 = (bf16[64,2048]{1,0:T(8,128)(2,1)S(1)}, bf16[64,2048]{1,0:T(8,128)(2,1)}, u32[]{:S(2)}) copy-start(bf16[64,2048]{1,0:T(8,128)(2,1)} %param.25) | copy-start | bytes 786436
  283.6 14.3 %copy-start.4 = (f32[2048]{0:T(1024)S(1)}, f32[2048]{0:T(1024)}, u32[]{:S(2)}) copy-start(f32[2048]{0:T(1024)} %param.27) | copy-start | bytes 24580
  285.0 8.9 %all-to-all-start = ((bf16[4,64,256]{2,1,0:T(8,128)(2,1)}), bf16[4,64,256]{2,1,0:T(8,128)(2,1)S(1)}, u32[]{:S(2)}, u32[]{:S(2)}) async-start(bf16[4,64,256]{2,1,0:T(8,128)(2,1)} %all_to_all.20), calls=%async_computation | async-start | bytes 262144 | tf_op jit(solution)/shard_map/all_to_all | solution.py:100
  289.0 96.2 %all-gather.5.cloned.1.call-start = ((), (), s32[]{:S(2)}) async-start(), calls=%async_computation.5 | async-start | bytes 5242880 | tf_op jit(solution)/shard_map/all_gather | solution.py:130
  297.0 0.9 copy-start.1
  339.4 107.3 %reduce-scatter.2.cloned.1.call-start = ((), (), s32[]{:S(2)}) async-start(), calls=%async_computation.6 | async-start | bytes 5242880 | tf_op jit(solution)/shard_map/reduce_scatter | solution.py:135
  396.6 64.3 %copy-start.5 = (s32[64,2]{0,1:T(2,128)S(1)}, s32[64,2]{0,1:T(2,128)}, u32[]{:S(2)}) copy-start(s32[64,2]{0,1:T(2,128)} %param.28) | copy-start | bytes 1540
  396.6 64.6 %copy-start.3 = (f32[64,2]{0,1:T(2,128)S(1)}, f32[64,2]{0,1:T(2,128)}, u32[]{:S(2)}) copy-start(f32[64,2]{0,1:T(2,128)} %param.29) | copy-start | bytes 1540
  396.7 64.6 %copy-start.7 = (f32[64]{0:T(128)S(1)}, f32[64]{0:T(128)}, u32[]{:S(2)}) copy-start(f32[64]{0:T(128)} %param.30) | copy-start | bytes 772
  450.1 39.0 %all-to-all-start.2 = ((bf16[128,2,2048]{2,1,0:T(2,128)(2,1)}), bf16[128,2,2048]{2,1,0:T(2,128)(2,1)}, u32[]{:S(2)}, u32[]{:S(2)}) async-start(bf16[128,2,2048]{2,1,0:T(2,128)(2,1)} %bitcast.14), calls=%async_computation.3 | async-start | bytes 2097152 | tf_op jit(solution)/shard_map/all_to_all | solution.py:137
Sparse Core Ops, SparseCore 0:
  10.1 103.3 all-gather.2
  339.5 45.6 all-gather.4
  396.8 49.8 reduce-scatter.1
where the time goes:
time: 507 us; the launch traced here: 504 us
  waiting for transfers between devices  230 us (45%)
  local copies, waits for them, and re-layouts  127 us (25%)
  matrix products  64.3 us (13%)
  blocking collectives  35.5 us (7%)
  other arithmetic  17.7 us (3%)
  starting transfers between devices  15 us (3%)
  between operations  13.4 us (3%)
    all_gather x1, waiting for transfers between devices, sent_together(): whole = lax.all_gather(both, axis, axis=dim, tiled=True)  102 us
    reduce_scatter x1, waiting for transfers between devices, on_device(): lax.psum_scatter(part_sum.astype(jnp.bfloat16), 'tp', scatter_dimension=0...  50 us
    all_gather x1, waiting for transfers between devices, on_device(): everyone = lax.all_gather(grouped, 'tp', axis=0, tiled=True)  45.8 us
    unnamed x23, local copies, waits for them, and re-layouts  43.9 us
    all_to_all x1, blocking collectives, on_device(): lax.all_to_all(outgoing, 'sp', split_axis=0, concat_axis=0, tiled=True)  35.5 us
    dot_general x16, matrix products, absorb(): jnp.einsum('thd,shd->hts', queries, keys, preferred_element_type=jnp.floa...  29 us
    all_to_all x1, waiting for transfers between devices, on_device(): lax.all_to_all(answered, 'sp', split_axis=0, concat_axis=0, tiled=True)  27.6 us
    dot_general x16, matrix products, absorb(): jnp.einsum('hts,shd->htd', expo.astype(jnp.bfloat16), vals, preferred_ele...  19.2 us
  transfers between devices with their start and end apart: 5, of which 5 were waited for; matrix products, arithmetic and copies ran while one was open for 1% of the time, Pallas kernels for 0%

commit v1 on v0

v1 whole, which is shorter than its diff:
```python
import functools
import math

import jax
import jax.numpy as jnp
from jax import lax
from jax.experimental import pallas as pl
from jax.experimental.pallas import tpu as pltpu
from jax.sharding import PartitionSpec as P

norm_epsilon = 1e-06
MESH = pl.DeviceIdType.MESH
log2_e = math.log2(math.e)

NZ, NX = 8, 4
ROWS_A, ROWS_B = 96, 160
HALF_A, HALF_B = ROWS_A // 2, ROWS_B // 2
UNIT_ORDER = (0, 1, 7, 2, 6, 3, 5, 4)


def gather_plan():
    rate, lag = 46.6, 2.0
    ready, links, sends = {}, {}, []

    def rows_of(piece):
        kind, _, _, part = piece
        whole, half = (ROWS_A, HALF_A) if kind == "A" else (ROWS_B, HALF_B)
        return whole if part < 0 else half

    def follow(piece):
        kind, dz, slot, part = piece
        out = []
        if kind == "A":
            if dz == 0:
                if slot == 0:
                    out += [("x+", ("A", 0, 2, -1), -1), ("x-", ("A", 0, 1, -1), -1)]
                if slot == 2:
                    out.append(("x+", ("A", 0, 3, 0), 0))
                if slot == 1:
                    out.append(("x-", ("A", 0, 3, 1), 1))
                out += [("z+", ("A", 7, slot, part), part), ("z-", ("A", 1, slot, part), part)]
            elif dz in (7, 6) or (dz == 5 and slot < 2):
                out.append(("z+", ("A", dz - 1, slot, part), part))
            elif dz in (1, 2) or (dz == 3 and slot >= 2):
                out.append(("z-", ("A", dz + 1, slot, part), part))
            return out
        if slot == 0:
            if dz == 0:
                out += [("z+", ("B", 7, 0, -1), -1), ("z-", ("B", 1, 0, -1), -1)]
            elif dz in (7, 6):
                out.append(("z+", ("B", dz - 1, 0, -1), -1))
            elif dz in (1, 2):
                out.append(("z-", ("B", dz + 1, 0, -1), -1))
            elif dz == 5:
                out.append(("z+", ("B", 4, 0, 0), 0))
            elif dz == 3:
                out.append(("z-", ("B", 4, 0, 1), 1))
            out += [("x+", ("B", dz, 2, part), part), ("x-", ("B", dz, 1, part), part)]
        elif slot == 2 and dz < 4:
            out.append(("x+", ("B", dz, 3, part), part))
        elif slot == 1 and dz >= 4:
            out.append(("x-", ("B", dz, 3, part), part))
        return out

    events = [(0.0, 1, ("B", 0, 0, -1)), (0.0, 0, ("A", 0, 0, -1))]
    order = []
    while events:
        events.sort()
        now, _, piece = events.pop(0)
        order.append((now, piece, follow(piece)))
        for link, target, _ in follow(piece):
            begin = max(links.get(link, 0.0), now)
            links[link] = begin + rows_of(target) / rate
            events.append((links[link] + lag, len(order), target))
    return order


PLAN = gather_plan()
PIECES = [piece for _, piece, _ in PLAN]
PIECE_INDEX = {piece: n for n, piece in enumerate(PIECES)}
COMPUTE_US = 2.3


def unit_slots():
    units = [(kind, dz) for dz in UNIT_ORDER for kind in ("B", "A")]
    slots, clock, taken = [], 0.0, 0
    for kind, dz in units:
        need = max(t for t, piece, _ in PLAN if piece[0] == kind and piece[1] == dz) + 1.0
        clock = max(clock, need)
        mine = []
        while taken < len(PLAN) and PLAN[taken][0] <= clock:
            mine.append(taken)
            taken += 1
        slots.append(mine)
        clock += COMPUTE_US * (ROWS_A if kind == "A" else ROWS_B) / 128
    assert taken == len(PLAN)
    return units, slots


UNITS, SLOTS = unit_slots()


def attend_kernel(
    q1_ref, q2_ref, k1_ref, k2_ref, v_ref, lam_ref, gain_ref, gate_ref, up_ref, down_ref,
    out_ref, wg_ref, wu_ref, wd_ref, rg_ref, ru_ref, rd_ref,
    kva, kvb, qt, m_ref, l_ref, acc_ref, att,
    load_sem, send_sem, recv_sem, pass_sem, got_sem, head_send, head_recv,
    ws_sem, wr_sem, wl_sem, relay_sem, relay_send, pair_send, pair_recv,
):
    sp = lax.axis_index("sp")
    y = lax.axis_index("tp")
    core = lax.rem(sp, 2)
    x = lax.rem(sp // 2, NX)
    z = sp // (2 * NX)

    def place(zz, xx, cc):
        return (zz * NX + xx) * 2 + cc

    peers = {
        "x+": (place(z, lax.rem(x + 1, NX), core), y),
        "x-": (place(z, lax.rem(x + NX - 1, NX), core), y),
        "z+": (place(lax.rem(z + 1, NZ), x, core), y),
        "z-": (place(lax.rem(z + NZ - 1, NZ), x, core), y),
        "pair": (place(z, x, 1 - core), y),
        "y1": (sp, lax.rem(y + 1, 4)),
        "y2": (sp, lax.rem(y + 2, 4)),
        "y3": (sp, lax.rem(y + 3, 4)),
    }

    loads = []
    for n, (buf, low, high) in enumerate(((kvb, ROWS_A, 256), (kva, 0, ROWS_A))):
        for c, (ref, lo, hi) in enumerate(((k1_ref, 0, 128), (k2_ref, 128, 256), (v_ref, 256, 512))):
            copy = pltpu.make_async_copy(
                ref.at[low:high], buf.at[0, 0, 0, :, lo:hi], load_sem.at[n * 3 + c]
            )
            copy.start()
            loads.append(copy)

    barrier = pltpu.get_barrier_semaphore()
    for peer in peers.values():
        pl.semaphore_signal(barrier, inc=1, device_id=peer, device_id_type=MESH)
    pl.semaphore_wait(barrier, len(peers))

    def region(piece, side):
        kind, dz, slot, part = piece
        buf, half = (kva, HALF_A) if kind == "A" else (kvb, HALF_B)
        ref = buf.at[dz, side, slot]
        return ref if part < 0 else ref.at[part * half:(part + 1) * half]

    def part_of(piece, part):
        kind, dz, slot, own = piece
        return region(piece, 0) if part == own else region((kind, dz, slot, part), 0)

    def copy_on(piece, link, target, part):
        n = PIECE_INDEX[target]
        return pltpu.make_async_remote_copy(
            src_ref=part_of(piece, part), dst_ref=region(target, 0),
            send_sem=send_sem.at[n], recv_sem=recv_sem.at[n],
            device_id=peers[link], device_id_type=MESH,
        )

    def hand_over(piece):
        n = PIECE_INDEX[piece]
        return pltpu.make_async_remote_copy(
            src_ref=region(piece, 0), dst_ref=region(piece, 1),
            send_sem=pass_sem.at[n], recv_sem=got_sem.at[n],
            device_id=peers["pair"], device_id_type=MESH,
        )

    def arrive(piece):
        n = PIECE_INDEX[piece]
        pltpu.make_async_remote_copy(
            src_ref=region(piece, 0), dst_ref=region(piece, 0),
            send_sem=send_sem.at[n], recv_sem=recv_sem.at[n],
            device_id=peers["pair"], device_id_type=MESH,
        ).wait_recv()

    weights = ((gate_ref, wg_ref, rg_ref), (up_ref, wu_ref, ru_ref), (down_ref, wd_ref, rd_ref))
    home = y // 2 == core
    relay_plus = lax.rem(y + 1, 4) // 2 == core

    def half_of(ref, half):
        rows = ref.shape[0] // 2
        return ref.at[half * rows:(half + 1) * rows]

    def far_copy(a, j, half):
        src, _, relay = weights[a]
        return pltpu.make_async_remote_copy(
            src_ref=half_of(src.at[j], half), dst_ref=relay,
            send_sem=ws_sem.at[2 + half, a], recv_sem=relay_sem.at[a],
            device_id=peers["y1" if half == 0 else "y3"], device_id_type=MESH,
        )

    def near_copy(a, j, delta):
        src, dst, _ = weights[a]
        return pltpu.make_async_remote_copy(
            src_ref=src.at[j], dst_ref=dst.at[4 - delta],
            send_sem=ws_sem.at[0 if delta == 1 else 1, a], recv_sem=wr_sem.at[0 if delta == 3 else 1, a],
            device_id=peers["y1" if delta == 1 else "y3"], device_id_type=MESH,
        )

    def relay_copy(a, half):
        _, dst, relay = weights[a]
        return pltpu.make_async_remote_copy(
            src_ref=relay, dst_ref=half_of(dst.at[2], half),
            send_sem=relay_send.at[a], recv_sem=wr_sem.at[2 + half, a],
            device_id=peers["y1" if half == 0 else "y3"], device_id_type=MESH,
        )

    def own_copy(a, j):
        src, dst, _ = weights[a]
        return pltpu.make_async_copy(src.at[j], dst.at[0], wl_sem.at[a])

    def pair_copy(a, r):
        _, dst, _ = weights[a]
        return pltpu.make_async_remote_copy(
            src_ref=dst.at[r], dst_ref=dst.at[r],
            send_sem=pair_send.at[r, a], recv_sem=pair_recv.at[r, a],
            device_id=peers["pair"], device_id_type=MESH,
        )

    def each_delta(action, deltas):
        for j in range(2):
            delta_of = lax.rem(2 * core + j + 4 - y, 4)
            for delta in deltas:
                @pl.when(delta_of == delta)
                def _():
                    action(j, delta)

    def start_far(j, delta):
        for a in range(3):
            far_copy(a, j, 0).start()
            far_copy(a, j, 1).start()

    def start_near(j, delta):
        for a in range(3):
            near_copy(a, j, delta).start()

    def start_own(j, delta):
        for a in range(3):
            own_copy(a, j).start()

    def start_weights():
        each_delta(start_far, (2,))
        each_delta(start_near, (1, 3))
        each_delta(start_own, (0,))

    def relay_weights():
        for half in range(2):
            @pl.when(relay_plus if half == 0 else jnp.logical_not(relay_plus))
            def _():
                for a in range(3):
                    far_copy(a, 0, half).wait_recv()
                    relay_copy(a, half).start()

    def pass_near():
        @pl.when(home)
        def _():
            for a in range(3):
                own_copy(a, 0).wait()
                pair_copy(a, 0).start()
            for r in (1, 3):
                for a in range(3):
                    near_copy(a, 0, 4 - r).wait_recv()
                    pair_copy(a, r).start()

    def finish_weights():
        @pl.when(home)
        def _():
            for a in range(3):
                for half in range(2):
                    relay_copy(a, half).wait_recv()
                pair_copy(a, 2).start()
            for r in range(4):
                for a in range(3):
                    pair_copy(a, r).wait_send()

        @pl.when(jnp.logical_not(home))
        def _():
            for r in range(4):
                for a in range(3):
                    pair_copy(a, r).wait_recv()

        def drain_far(j, delta):
            for a in range(3):
                far_copy(a, j, 0).wait_send()
                far_copy(a, j, 1).wait_send()

        def drain_near(j, delta):
            for a in range(3):
                near_copy(a, j, delta).wait_send()

        each_delta(drain_far, (2,))
        each_delta(drain_near, (1, 3))
        for a in range(3):
            relay_copy(a, 0).wait_send()

    def handle(n):
        _, piece, onward = PLAN[n]
        own = piece[1] == 0 and piece[2] == 0
        if own:
            for copy in loads[0:3] if piece[0] == "B" else loads[3:6]:
                copy.wait()
        else:
            arrive(piece)
        for link, target, part in onward:
            copy_on(piece, link, target, part).start()
        hand_over(piece).start()

    owned = [n for n in range(len(PLAN)) if PLAN[n][1][1] == 0 and PLAN[n][1][2] == 0]
    for n in owned:
        handle(n)
    start_weights()

    for m, ref in enumerate((q1_ref, q2_ref)):
        flipped = (ref[...].astype(jnp.float32) * 0.125).T
        row = lax.broadcasted_iota(jnp.int32, flipped.shape, 0)
        for h in range(2):
            mine = (row >= 64 * h) & (row < 64 * (h + 1))
            qt[h, m] = jnp.where(mine, flipped, 0.0).astype(jnp.bfloat16)
    m_ref[...] = jnp.full(m_ref.shape, -1e30, jnp.float32)
    l_ref[...] = jnp.zeros(l_ref.shape, jnp.float32)
    acc_ref[...] = jnp.zeros(acc_ref.shape, jnp.float32)

    def compute(buf, dz):
        rows = buf.shape[1] * buf.shape[2] * buf.shape[3]
        for h in range(2):
            vals = buf[dz, :, :, :, 256 + 128 * h:384 + 128 * h].reshape(rows, 128)
            for m in range(2):
                keys = buf[dz, :, :, :, 128 * m:128 * (m + 1)].reshape(rows, 128)
                scores = jnp.dot(keys, qt[h, m], preferred_element_type=jnp.float32)
                i = h * 2 + m
                old = m_ref[i]
                new = jnp.maximum(old, jnp.max(scores, axis=0, keepdims=True))
                shrink = jnp.exp2((old - new) * log2_e)
                expo = jnp.exp2((scores - new) * log2_e)
                m_ref[i] = new
                l_ref[i] = l_ref[i] * shrink + jnp.sum(expo, axis=0, keepdims=True)
                acc_ref[i] = acc_ref[i] * shrink + lax.dot_general(
                    vals, expo.astype(jnp.bfloat16), (((0,), (0,)), ((), ())),
                    preferred_element_type=jnp.float32,
                )

    def step(t, carry):
        dz = jnp.where(lax.rem(t, 2) == 1, (t + 1) // 2, lax.rem(NZ - (t + 1) // 2, NZ))
        for side, (kind, buf) in enumerate((("B", kvb), ("A", kva))):
            for i in range(NZ):
                u = 2 * i + side

                @pl.when(t == i)
                def _():
                    for n in SLOTS[u]:
                        if n not in owned:
                            handle(n)
                    for piece in PIECES:
                        if (piece[0], piece[1]) == UNITS[u]:
                            hand_over(piece).wait_recv()
                    if u == 7:
                        relay_weights()
                    if u == 13:
                        pass_near()
            compute(buf, dz)
        return carry

    lax.fori_loop(0, NZ, step, 0)

    for h in range(2):
        one = acc_ref[2 * h] / l_ref[2 * h]
        two = acc_ref[2 * h + 1] / l_ref[2 * h + 1]
        joined = one - lam_ref[h] * two
        scale = lax.rsqrt(jnp.mean(joined * joined, axis=0, keepdims=True) + norm_epsilon)
        joined = joined * scale * gain_ref[...]
        att[:, :, 128 * h:128 * (h + 1)] = joined.T.astype(jnp.bfloat16).reshape(4, 64, 128)

    keep = pltpu.make_async_copy(att.at[y], out_ref.at[y], head_recv.at[0])
    keep.start()

    def head_copy(d):
        return pltpu.make_async_remote_copy(
            src_ref=att.at[lax.rem(y + d, 4)], dst_ref=out_ref.at[y],
            send_sem=head_send.at[d], recv_sem=head_recv.at[d],
            device_id=peers[f"y{d}"], device_id_type=MESH,
        )

    for d in (2, 1, 3):
        head_copy(d).start()
    finish_weights()
    for d in (1, 2, 3):
        head_copy(d).wait()
    keep.wait()
    for n, piece in enumerate(PIECES):
        hand_over(piece).wait_send()
        for link, target, part in PLAN[n][2]:
            copy_on(piece, link, target, part).wait_send()


def attend(q1, q2, k1, k2, v, lam, gain, gate, up, down):
    n = len(PIECES)
    bf16 = jnp.bfloat16
    dma = pltpu.SemaphoreType.DMA
    vmem = pl.BlockSpec(memory_space=pltpu.VMEM)
    hbm = pl.BlockSpec(memory_space=pl.ANY)
    _, d, f = gate.shape
    shapes = (
        (4, 64, 256), (4, d, f), (4, d, f), (4, f, d), (d // 2, f), (d // 2, f), (f // 2, d),
    )
    return pl.pallas_call(
        attend_kernel,
        out_shape=[jax.ShapeDtypeStruct(s, bf16) for s in shapes],
        in_specs=[vmem, vmem, hbm, hbm, hbm, pl.BlockSpec(memory_space=pltpu.SMEM), vmem, hbm, hbm, hbm],
        out_specs=[hbm] * 7,
        scratch_shapes=[
            pltpu.VMEM((NZ, 2, 4, ROWS_A, 512), bf16),
            pltpu.VMEM((NZ, 2, 4, ROWS_B, 512), bf16),
            pltpu.VMEM((2, 2, 128, 256), bf16),
            pltpu.VMEM((4, 1, 256), jnp.float32),
            pltpu.VMEM((4, 1, 256), jnp.float32),
            pltpu.VMEM((4, 128, 256), jnp.float32),
            pltpu.VMEM((4, 64, 256), bf16),
            dma((6,)), dma((n,)), dma((n,)), dma((n,)), dma((n,)), dma((4,)), dma((4,)),
            dma((4, 3)), dma((4, 3)), dma((3,)), dma((3,)), dma((3,)), dma((4, 3)), dma((4, 3)),
        ],
        compiler_params=pltpu.CompilerParams(
            collective_id=0, has_side_effects=True, vmem_limit_bytes=60 * 1024 * 1024
        ),
        name="gather_attend",
    )(q1, q2, k1, k2, v, lam, gain, gate, up, down)


def on_device(
    query_one, key_one, query_two, key_two, values, mix_lambda, head_gain, residual_in, out_weight,
    norm_gain, route_ids, route_logits, group_prob, gate_weight, up_weight, down_weight,
):
    heads, wg, wu, wd, _, _, _ = attend(
        query_one, query_two, key_one, key_two, values, mix_lambda, head_gain.reshape(128, 1),
        gate_weight, up_weight, down_weight,
    )
    share, width = residual_in.shape
    top_count = route_ids.shape[1]
    device_count = lax.axis_size("sp") * lax.axis_size("tp")
    token_heads = heads.transpose(1, 0, 2).reshape(share, -1)
    mix = jnp.dot(token_heads, out_weight, preferred_element_type=jnp.float32)
    hidden_f = (residual_in.astype(jnp.float32) + mix).astype(jnp.bfloat16).astype(jnp.float32)
    normed = (
        hidden_f
        * lax.rsqrt(jnp.mean(hidden_f * hidden_f, axis=-1, keepdims=True) + norm_epsilon)
        * norm_gain
    ).astype(jnp.bfloat16)

    flat_ids = route_ids.reshape(-1)
    same = flat_ids[:, None] == flat_ids[None, :]
    count = flat_ids.shape[0]
    before = jnp.arange(count)[None, :] < jnp.arange(count)[:, None]
    rank = jnp.sum((same & before).astype(jnp.int32), axis=1)
    slot_of = ((flat_ids // 4) * 2 + rank) * 4 + flat_ids % 4
    pair_slots = slot_of.reshape(share, top_count)
    places = jnp.arange(device_count, dtype=jnp.int32)
    table = jnp.zeros((device_count, share), jnp.bool_)
    for k in range(top_count):
        table = table | (places[:, None] == pair_slots[None, :, k])
    outgoing = jnp.dot(table.astype(jnp.bfloat16), normed, preferred_element_type=jnp.float32)
    outgoing = outgoing.astype(jnp.bfloat16)
    arrived = lax.all_to_all(outgoing, ("sp", "tp"), 0, 0, tiled=True)
    gate = jnp.einsum("sd,rdf->rsf", arrived, wg, preferred_element_type=jnp.float32)
    upper = jnp.einsum("sd,rdf->rsf", arrived, wu, preferred_element_type=jnp.float32)
    middle = (jax.nn.silu(gate) * upper).astype(jnp.bfloat16)
    parts = jnp.einsum("rsf,rfd->rsd", middle, wd, preferred_element_type=jnp.float32)
    answered = jnp.sum(parts.astype(jnp.bfloat16).astype(jnp.float32), axis=0).astype(jnp.bfloat16)
    returned = lax.all_to_all(answered, ("sp", "tp"), 0, 0, tiled=True)
    picked = returned[slot_of].astype(jnp.float32).reshape(share, top_count, width)
    route_weight = jax.nn.softmax(route_logits, axis=-1) * group_prob[:, None]
    moe = jnp.sum(picked * route_weight[..., None], axis=1)
    return (hidden_f + moe).astype(jnp.bfloat16)


def solution(mesh):
    in_specs = (
        P("sp", "tp"), P("sp", "tp"), P("sp", "tp"), P("sp", "tp"), P("sp", "tp"), P("tp"), P(),
        P(("sp", "tp"), None), P(), P(), P(("sp", "tp"), None), P(("sp", "tp"), None), P(("sp", "tp")),
        P("sp", None, "tp"), P("sp", None, "tp"), P("sp", "tp", None),
    )
    return jax.shard_map(
        on_device, mesh=mesh, in_specs=in_specs, out_specs=P(("sp", "tp"), None), check_vma=False
    )
```

time: 507 us -> 240 us (0.47)
  waiting for transfers between devices: 230 us -> 30.5 us
  Pallas kernels: 0 us -> 125 us
  local copies, waits for them, and re-layouts: 127 us -> 14.1 us
  matrix products: 64.3 us -> 17.4 us
  between operations: 13.4 us -> 0.21 us
  other arithmetic: 17.7 us -> 6.12 us
  starting transfers between devices: 15 us -> 6.63 us
    all_gather x2 -> x0, waiting for transfers between devices: 148 us -> none  [the longest x1 102 us: sent_together(): whole = lax.all_gather(both, axis, axis=dim, tiled=True)]
    pallas_call x0 -> x1, Pallas kernels: none -> 125 us  [attend(): pl.pallas_call(attend_kernel, out_shape=[jax.ShapeDtypeStruct(s, bf16) fo...]
    reduce_scatter x1 -> x0, waiting for transfers between devices: 50 us -> none  [on_device(): lax.psum_scatter(part_sum.astype(jnp.bfloat16), 'tp', scatter_dimension=0...]
    dot_general x35 -> x3, matrix products: 61.1 us -> 14.2 us  [the longest x1 8.35 us: on_device(): jnp.einsum('rsf,rfd->rsd', middle, wd, preferred_element_type=jnp.float32)]
    reshape x7 -> x2, local copies, waits for them, and re-layouts: 47.5 us -> 2.31 us  [the longest x1 1.39 us: on_device(): head_gain.reshape(128, 1)]
    unnamed x23 -> x20, local copies, waits for them, and re-layouts: 43.9 us -> 8.89 us
    dynamic_slice x8 -> x0, local copies, waits for them, and re-layouts: 14.5 us -> none  [on_device(): folded, _ = lax.scan(advance, folded, blocks)]
    split x2 -> x0, local copies, waits for them, and re-layouts: 12.8 us -> none  [sent_together(): jnp.split(whole, [sum(widths[:k]) for k in range(1, len(widths))], axis=a...]
  transfers between devices with their start and end apart: 5 -> 1, of which waited for: 5 -> 1; matrix products, arithmetic and copies ran while one was open for 1% -> 0% of each run, Pallas kernels for 0% -> 0%
where the time goes in v1:
time: 240 us
  Pallas kernels  125 us (52%)
  blocking collectives  40 us (17%)
  waiting for transfers between devices  30.5 us (13%)
  matrix products  17.4 us (7%)
  local copies, waits for them, and re-layouts  14.1 us (6%)
  starting transfers between devices  6.63 us (3%)
  other arithmetic  6.12 us (3%)
    pallas_call x1, Pallas kernels, attend(): pl.pallas_call(attend_kernel, out_shape=[jax.ShapeDtypeStruct(s, bf16) fo...  125 us
    all_to_all x1, blocking collectives, on_device(): arrived = lax.all_to_all(outgoing, ('sp', 'tp'), 0, 0, tiled=True)  40 us
    all_to_all x1, waiting for transfers between devices, on_device(): returned = lax.all_to_all(answered, ('sp', 'tp'), 0, 0, tiled=True)  30.5 us
    unnamed x20, local copies, waits for them, and re-layouts  8.89 us
    dot_general x1, matrix products, on_device(): jnp.einsum('rsf,rfd->rsd', middle, wd, preferred_element_type=jnp.float32)  8.35 us
    all_to_all x1, starting transfers between devices, on_device(): returned = lax.all_to_all(answered, ('sp', 'tp'), 0, 0, tiled=True)  6.63 us
    dot_general x1, matrix products, on_device(): jnp.einsum('sd,rdf->rsf', arrived, wg, preferred_element_type=jnp.float32)  5.36 us
  transfers between devices with their start and end apart: 1, of which 1 were waited for; matrix products, arithmetic and copies ran while one was open for 0% of the time, Pallas kernels for 0%

profile of v1, /device:TPU:1, one launch (start us, length us, event | category | flops | bytes accessed | tf_op | source)
XLA Modules:
  0.0 239.6 jit_solution(5320606357086782084)
XLA Ops:
  0.0 0.0 copy-start.3
  0.0 0.8 copy.79
  0.8 0.7 broadcast_compare_fusion
  1.5 1.4 copy.77.gain_ref
  2.9 124.6 %gather_attend.1 = (bf16[4,64,256]{2,1,0:T(8,128)(2,1)}, bf16[4,2048,256]{2,1,0:T(8,128)(2,1)}, bf16[4,2048,256]{2,1,0:T(8,128)(2,1)}, bf16[4,256,2048]{2,1,0:T(...) custom-call(bf16[256,128]{1,0:T(8,128)(2,1)} %q1_ref.1, ...), custom_call_target="tpu_custom_call" | custom-call | tf_op jit(solution)/shard_map/gather_attend/pallas_call | solution.py:407
  127.5 0.0 copy-start.5
  127.5 0.9 copy.100
  128.4 0.0 copy-done.3
  128.4 3.2 %multiply_reduce_fusion.1 = (f32[64]{0:T(128)S(1)}, f32[64,2048]{1,0:T(8,128)S(1)}) fusion(bf16[64,1024]{1,0:T(8,128)(2,1)S(1)} %bitcast.44, bf16[1024,2048]{1,0:T(8,128)(2,1)} %param.24, bf16[64,2048]{1,0:T(8,128)(2,1)S(1)} %copy-done.3), kind=kOutput, calls=%fused_computation.18 | convolution fusion | flops 269221824 | bytes 5112064 | tf_op jit(solution)/shard_map/dot_general | solution.py:442
  131.6 0.0 copy-start
  131.6 0.1 eq.48
  131.8 0.2 convert_reduce_fusion.1
  131.9 0.1 reduce_sum.53
  132.1 0.1 copy.84
  132.3 0.2 slice_reduce_fusion.1
  132.4 0.0 copy-done.5
  132.4 0.5 fusion
  132.9 0.5 broadcast.149
  133.4 1.4 reduce.5
  134.9 1.6 reshape.172
  136.5 40.0 %all_to_all.24 = bf16[256,2,1024]{2,1,0:T(2,128)(2,1)S(1)} all-to-all(bf16[256,2,1024]{2,1,0:T(2,128)(2,1)} %reshape.172), channel_id=1, replica_groups=mesh['sp'=64,'tp'=4] {'sp','tp'}, dimensions={0} | all-to-all | bytes 2097152 | tf_op jit(solution)/shard_map/all_to_all | solution.py:463
  176.5 3.3 %reshape.173 = bf16[256,1,2048]{2,1,0:T(2,128)(2,1)} reshape(bf16[256,2,1024]{2,1,0:T(2,128)(2,1)S(1)} %all_to_all.24) | data formatting | bytes 2097152
  179.9 0.0 copy-done
  179.9 0.0 copy-start.2
  179.9 5.4 %convolution_bitcast_fusion.1 = f32[4,256,256]{1,2,0:T(8,128)} fusion(bf16[4,2048,256]{2,1,0:T(8,128)(2,1)} %get-tuple-element.10, bf16[256,1,2048]{2,1,0:T(2,128)(2,1)} %reshape.173), kind=kOutput, calls=%fused_computation.9 | convolution fusion | flops 1073741824 | bytes 6291456 | tf_op jit(solution)/shard_map/sd,rdf->rsf/dot_general | solution.py:464
  185.2 0.0 copy-done.2
  185.2 8.4 %convert_reduce_fusion = bf16[256,2048]{1,0:T(8,128)(2,1)S(1)} fusion(bf16[4,256,2048]{2,1,0:T(8,128)(2,1)} %get-tuple-element.12, bf16[4,2048,256]{2,1,0:T(8,128)(2,1)} %get-tuple-element.11, f32[4,256,256]{1,2,0:T(8,128)} %convolution_bitcast_fusion.1, bf16[256,1,2048]{2,1,0:T(2,128)(2,1)S(1)} %copy-done.2), kind=kOutput, calls=%fused_computation.1 | convolution fusion | flops 2152726528 | bytes 11534336 | tf_op jit(solution)/shard_map/rsf,rfd->rsd/dot_general | solution.py:467
  193.6 0.0 copy-start.4
  193.6 0.0 copy-start.6
  193.6 1.4 reduce.6
  195.1 1.6 reshape.174
  196.7 6.6 %all-to-all-start.1 = ((bf16[256,2,1024]{2,1,0:T(2,128)(2,1)}), bf16[256,2,1024]{2,1,0:T(2,128)(2,1)S(1)}, u32[]{:S(2)}, u32[]{:S(2)}) async-start(bf16[256,2,1024]{2,1,0:T(2,128)(2,1)} %reshape.174), calls=%async_computation.1 | async-start | bytes 2097152 | tf_op jit(solution)/shard_map/all_to_all | solution.py:469
  203.3 0.1 reshape.158
  203.4 0.0 copy-done.4
  203.5 0.0 copy-done.6
  203.5 0.1 copy.93
  203.6 30.5 %all-to-all-done.1 = bf16[256,2,1024]{2,1,0:T(2,128)(2,1)S(1)} async-done(((bf16[256,2,1024]{2,1,0:T(2,128)(2,1)}), bf16[256,2,1024]{2,1,0:T(2,128)(2,1)S(1)}, u32[]{:S(2)}, u32[]{:S(2)}) %all-to-all-start.1) | async-done | bytes 1048608 | tf_op jit(solution)/shard_map/all_to_all | solution.py:469
  234.1 0.9 reshape.175
  235.0 0.6 copy.111
  235.6 0.0 copy-start.1
  235.6 0.9 gather_fusion
  236.6 0.7 reshape.159
  237.2 1.5 multiply_reduce_fusion
  238.8 0.0 copy-done.1
  238.8 0.8 add_convert_fusion
  (7 shorter events, 0.1 us)
Async XLA Ops:
  0.0 128.4 %copy-start.3 = (bf16[64,2048]{1,0:T(8,128)(2,1)S(1)}, bf16[64,2048]{1,0:T(8,128)(2,1)}, u32[]{:S(2)}) copy-start(bf16[64,2048]{1,0:T(8,128)(2,1)} %param.23) | copy-start | bytes 786436
  127.5 4.9 %copy-start.5 = (f32[2048]{0:T(1024)S(1)}, f32[2048]{0:T(1024)}, u32[]{:S(2)}) copy-start(f32[2048]{0:T(1024)} %param.25) | copy-start | bytes 24580
  131.6 48.3 %copy-start = (f32[64,2048]{1,0:T(8,128)}, f32[64,2048]{1,0:T(8,128)S(1)}, u32[]{:S(2)}) copy-start(f32[64,2048]{1,0:T(8,128)S(1)} %get-tuple-element.16) | copy-start | bytes 1572868
  179.9 5.4 %copy-start.2 = (bf16[256,1,2048]{2,1,0:T(2,128)(2,1)S(1)}, bf16[256,1,2048]{2,1,0:T(2,128)(2,1)}, u32[]{:S(2)}) copy-start(bf16[256,1,2048]{2,1,0:T(2,128)(2,1)} %reshape.173) | copy-start | bytes 3145732
  193.6 9.8 %copy-start.4 = (f32[64,2]{0,1:T(2,128)S(1)}, f32[64,2]{0,1:T(2,128)}, u32[]{:S(2)}) copy-start(f32[64,2]{0,1:T(2,128)} %param.27) | copy-start | bytes 1540
  193.6 9.9 %copy-start.6 = (f32[64]{0:T(128)S(1)}, f32[64]{0:T(128)}, u32[]{:S(2)}) copy-start(f32[64]{0:T(128)} %param.28) | copy-start | bytes 772
  196.7 37.5 %all-to-all-start.1 = ((bf16[256,2,1024]{2,1,0:T(2,128)(2,1)}), bf16[256,2,1024]{2,1,0:T(2,128)(2,1)S(1)}, u32[]{:S(2)}, u32[]{:S(2)}) async-start(bf16[256,2,1024]{2,1,0:T(2,128)(2,1)} %reshape.174), calls=%async_computation.1 | async-start | bytes 2097152 | tf_op jit(solution)/shard_map/all_to_all | solution.py:469
  235.6 3.2 %copy-start.1 = (f32[64,2048]{1,0:T(8,128)S(1)}, f32[64,2048]{1,0:T(8,128)}, u32[]{:S(2)}) copy-start(f32[64,2048]{1,0:T(8,128)} %copy-done) | copy-start | bytes 1572868

commit v2 on v1

--- a/solution.py
+++ b/solution.py
@@ -103,7 +103,7 @@
 def attend_kernel(
     q1_ref, q2_ref, k1_ref, k2_ref, v_ref, lam_ref, gain_ref, gate_ref, up_ref, down_ref,
     out_ref, wg_ref, wu_ref, wd_ref, rg_ref, ru_ref, rd_ref,
-    kva, kvb, qt, m_ref, l_ref, acc_ref, att,
+    kva, kvb, qt, m_ref, l_ref, acc_ref, att, own_gate, own_up, own_down,
     load_sem, send_sem, recv_sem, pass_sem, got_sem, head_send, head_recv,
     ws_sem, wr_sem, wl_sem, relay_sem, relay_send, pair_send, pair_recv,
 ):
@@ -207,14 +207,18 @@
             device_id=peers["y1" if half == 0 else "y3"], device_id_type=MESH,
         )
 
-    def own_copy(a, j):
-        src, dst, _ = weights[a]
-        return pltpu.make_async_copy(src.at[j], dst.at[0], wl_sem.at[a])
+    bounce = (own_gate, own_up, own_down)
+
+    def own_load(a, j):
+        return pltpu.make_async_copy(weights[a][0].at[j], bounce[a], wl_sem.at[0, a])
+
+    def own_store(a):
+        return pltpu.make_async_copy(bounce[a], weights[a][1].at[0], wl_sem.at[1, a])
 
     def pair_copy(a, r):
         _, dst, _ = weights[a]
         return pltpu.make_async_remote_copy(
-            src_ref=dst.at[r], dst_ref=dst.at[r],
+            src_ref=bounce[a] if r == 0 else dst.at[r], dst_ref=dst.at[r],
             send_sem=pair_send.at[r, a], recv_sem=pair_recv.at[r, a],
             device_id=peers["pair"], device_id_type=MESH,
         )
@@ -238,7 +242,7 @@
 
     def start_own(j, delta):
         for a in range(3):
-            own_copy(a, j).start()
+            own_load(a, j).start()
 
     def start_weights():
         each_delta(start_far, (2,))
@@ -253,12 +257,17 @@
                     far_copy(a, 0, half).wait_recv()
                     relay_copy(a, half).start()
 
+    def pass_own():
+        @pl.when(home)
+        def _():
+            for a in range(3):
+                own_load(a, 0).wait()
+                own_store(a).start()
+                pair_copy(a, 0).start()
+
     def pass_near():
         @pl.when(home)
         def _():
-            for a in range(3):
-                own_copy(a, 0).wait()
-                pair_copy(a, 0).start()
             for r in (1, 3):
                 for a in range(3):
                     near_copy(a, 0, 4 - r).wait_recv()
@@ -271,8 +280,9 @@
                 for half in range(2):
                     relay_copy(a, half).wait_recv()
                 pair_copy(a, 2).start()
-            for r in range(4):
-                for a in range(3):
+            for a in range(3):
+                own_store(a).wait()
+                for r in range(4):
                     pair_copy(a, r).wait_send()
 
         @pl.when(jnp.logical_not(home))
@@ -355,6 +365,8 @@
                     for piece in PIECES:
                         if (piece[0], piece[1]) == UNITS[u]:
                             hand_over(piece).wait_recv()
+                    if u == 0:
+                        pass_own()
                     if u == 7:
                         relay_weights()
                     if u == 13:
@@ -417,14 +429,175 @@
             pltpu.VMEM((4, 1, 256), jnp.float32),
             pltpu.VMEM((4, 128, 256), jnp.float32),
             pltpu.VMEM((4, 64, 256), bf16),
+            pltpu.VMEM((d, f), bf16), pltpu.VMEM((d, f), bf16), pltpu.VMEM((f, d), bf16),
             dma((6,)), dma((n,)), dma((n,)), dma((n,)), dma((n,)), dma((4,)), dma((4,)),
-            dma((4, 3)), dma((4, 3)), dma((3,)), dma((3,)), dma((3,)), dma((4, 3)), dma((4, 3)),
+            dma((4, 3)), dma((4, 3)), dma((2, 3)), dma((3,)), dma((3,)), dma((4, 3)), dma((4, 3)),
         ],
         compiler_params=pltpu.CompilerParams(
             collective_id=0, has_side_effects=True, vmem_limit_bytes=60 * 1024 * 1024
         ),
         name="gather_attend",
     )(q1, q2, k1, k2, v, lam, gain, gate, up, down)
+
+
+def expert_kernel(
+    heads_ref, resid_ref, proj_ref, norm_ref, pair_ref, slot_ref, weight_ref, wg_ref, wu_ref, wd_ref,
+    out_ref,
+    proj, vg, vu, vd, spread, outgoing, arrived, rows, total, answer, returned, hidden,
+    load_sem, go_sem, come_sem, back_sem, return_sem,
+):
+    sp = lax.axis_index("sp")
+    y = lax.axis_index("tp")
+    core = lax.rem(sp, 2)
+    x = lax.rem(sp // 2, NX)
+    z = sp // (2 * NX)
+    here = sp * 4 + y
+    devices = outgoing.shape[0]
+    group = devices // 2
+
+    loads = [pltpu.make_async_copy(proj_ref, proj, load_sem.at[3])]
+    for n, (src, dst) in enumerate(((wg_ref, vg), (wu_ref, vu), (wd_ref, vd))):
+        loads.append(pltpu.make_async_copy(src, dst, load_sem.at[n]))
+    for load in loads:
+        load.start()
+
+    def offset(i, sign):
+        dz, dy, dx, dc = lax.rem(i, NZ), lax.rem(i // NZ, 4), lax.rem(i // (4 * NZ), NX), i // group
+        zz = lax.rem(z + sign * dz + NZ, NZ)
+        xx = lax.rem(x + sign * dx + NX, NX)
+        yy = lax.rem(y + sign * dy + 4, 4)
+        cc = lax.rem(core + dc, 2)
+        return (zz * NX + xx) * 2 + cc, yy
+
+    barrier = pltpu.get_barrier_semaphore()
+
+    def greet(i, carry):
+        pl.semaphore_signal(barrier, inc=1, device_id=offset(i, 1), device_id_type=MESH)
+        return carry
+
+    lax.fori_loop(1, devices, greet, 0)
+
+    loads[0].wait()
+    mix = jnp.dot(heads_ref[0], proj[0], preferred_element_type=jnp.float32)
+    for t in range(1, 4):
+        mix = mix + jnp.dot(heads_ref[t], proj[t], preferred_element_type=jnp.float32)
+    kept = (resid_ref[...].astype(jnp.float32) + mix).astype(jnp.bfloat16).astype(jnp.float32)
+    scale = lax.rsqrt(jnp.mean(kept * kept, axis=-1, keepdims=True) + norm_epsilon)
+    normed = (kept * scale * norm_ref[...]).astype(jnp.bfloat16)
+    place = lax.broadcasted_iota(jnp.int32, (devices, kept.shape[0]), 0)
+    table = ((place == pair_ref[0:1, :]) | (place == pair_ref[1:2, :])).astype(jnp.bfloat16)
+    for k in range(16):
+        cols = slice(128 * k, 128 * (k + 1))
+        hidden[:, k, :] = kept[:, cols]
+        spread[:, k, :] = jnp.dot(table, normed[:, cols], preferred_element_type=jnp.float32)
+    outgoing[...] = spread[...].astype(jnp.bfloat16)
+    arrived[0] = outgoing[here]
+
+    pl.semaphore_wait(barrier, devices - 1)
+
+    def send(i, carry):
+        sp_to, y_to = offset(i, 1)
+        pltpu.make_async_remote_copy(
+            src_ref=outgoing.at[sp_to * 4 + y_to], dst_ref=arrived.at[i],
+            send_sem=go_sem.at[0], recv_sem=come_sem.at[i // group],
+            device_id=(sp_to, y_to), device_id_type=MESH,
+        ).start()
+        return carry
+
+    lax.fori_loop(1, devices, send, 0)
+
+    def whole(ref, low, high, send_sem, recv_sem):
+        return pltpu.make_async_remote_copy(
+            src_ref=ref.at[low:high], dst_ref=ref.at[low:high], send_sem=send_sem, recv_sem=recv_sem,
+            device_id=(sp, lax.rem(y + 1, 4)), device_id_type=MESH,
+        )
+
+    for load in loads[1:]:
+        load.wait()
+
+    def work(g, carry):
+        for n in range(2):
+            @pl.when(g == n)
+            def _():
+                whole(arrived, 1 - n, group, go_sem.at[0], come_sem.at[n]).wait_recv()
+        block = pl.ds(pl.multiple_of(g * group, group), group)
+        spread[0:group] = arrived[block].astype(jnp.float32)
+        for k in range(16):
+            rows[:, 128 * k:128 * (k + 1)] = spread[0:group, k, :].astype(jnp.bfloat16)
+        for r in range(4):
+            gate = jnp.dot(rows[...], vg[r], preferred_element_type=jnp.float32)
+            upper = jnp.dot(rows[...], vu[r], preferred_element_type=jnp.float32)
+            middle = (gate / (1.0 + jnp.exp(-gate)) * upper).astype(jnp.bfloat16)
+            part = jnp.dot(middle, vd[r], preferred_element_type=jnp.float32)
+            part = part.astype(jnp.bfloat16).astype(jnp.float32)
+            if r == 0:
+                total[...] = part
+            else:
+                total[...] = total[...] + part
+        for k in range(16):
+            spread[0:group, k, :] = total[:, 128 * k:128 * (k + 1)]
+        answer[block] = spread[0:group].astype(jnp.bfloat16)
+
+        def reply(i, inner):
+            sp_to, y_to = offset(i, -1)
+            pltpu.make_async_remote_copy(
+                src_ref=answer.at[i], dst_ref=returned.at[here],
+                send_sem=back_sem.at[0], recv_sem=return_sem.at[0],
+                device_id=(sp_to, y_to), device_id_type=MESH,
+            ).start()
+            return inner
+
+        lax.fori_loop(jnp.maximum(g * group, 1), (g + 1) * group, reply, 0)
+        return carry
+
+    lax.fori_loop(0, 2, work, 0)
+    returned[here] = answer[0]
+    whole(returned, 0, devices - 1, back_sem.at[0], return_sem.at[0]).wait_recv()
+
+    def combine(t, carry):
+        joined = hidden[t]
+        for k in range(2):
+            joined = joined + returned[slot_ref[2 * t + k]].astype(jnp.float32) * weight_ref[2 * t + k]
+        out_ref[t] = joined.astype(jnp.bfloat16)
+        return carry
+
+    lax.fori_loop(0, out_ref.shape[0], combine, 0)
+    whole(outgoing, 0, devices - 1, go_sem.at[0], come_sem.at[0]).wait_send()
+    whole(answer, 0, devices - 1, back_sem.at[0], return_sem.at[0]).wait_send()
+
+
+def run_experts(heads, resid, proj, norm, pair_slots, slots, route_weight, wg, wu, wd):
+    bf16, f32 = jnp.bfloat16, jnp.float32
+    dma = pltpu.SemaphoreType.DMA
+    vmem = pl.BlockSpec(memory_space=pltpu.VMEM)
+    smem = pl.BlockSpec(memory_space=pltpu.SMEM)
+    hbm = pl.BlockSpec(memory_space=pl.ANY)
+    share, width = resid.shape
+    devices = lax.axis_size("sp") * lax.axis_size("tp")
+    tiles = (width // 128, 128)
+    return pl.pallas_call(
+        expert_kernel,
+        out_shape=jax.ShapeDtypeStruct((share,) + tiles, bf16),
+        in_specs=[vmem, vmem, hbm, vmem, vmem, smem, smem, hbm, hbm, hbm],
+        out_specs=vmem,
+        scratch_shapes=[
+            pltpu.VMEM(proj.shape, bf16),
+            pltpu.VMEM(wg.shape, bf16), pltpu.VMEM(wu.shape, bf16), pltpu.VMEM(wd.shape, bf16),
+            pltpu.VMEM((devices,) + tiles, f32),
+            pltpu.VMEM((devices,) + tiles, bf16),
+            pltpu.VMEM((devices,) + tiles, bf16),
+            pltpu.VMEM((devices // 2, width), bf16),
+            pltpu.VMEM((devices // 2, width), f32),
+            pltpu.VMEM((devices,) + tiles, bf16),
+            pltpu.VMEM((devices,) + tiles, bf16),
+            pltpu.VMEM((share,) + tiles, f32),
+            dma((4,)), dma((1,)), dma((2,)), dma((1,)), dma((1,)),
+        ],
+        compiler_params=pltpu.CompilerParams(
+            collective_id=1, has_side_effects=True, vmem_limit_bytes=48 * 1024 * 1024
+        ),
+        name="experts",
+    )(heads, resid, proj, norm, pair_slots, slots, route_weight, wg, wu, wd)
 
 
 def on_device(
@@ -436,41 +609,18 @@
         gate_weight, up_weight, down_weight,
     )
     share, width = residual_in.shape
-    top_count = route_ids.shape[1]
-    device_count = lax.axis_size("sp") * lax.axis_size("tp")
-    token_heads = heads.transpose(1, 0, 2).reshape(share, -1)
-    mix = jnp.dot(token_heads, out_weight, preferred_element_type=jnp.float32)
-    hidden_f = (residual_in.astype(jnp.float32) + mix).astype(jnp.bfloat16).astype(jnp.float32)
-    normed = (
-        hidden_f
-        * lax.rsqrt(jnp.mean(hidden_f * hidden_f, axis=-1, keepdims=True) + norm_epsilon)
-        * norm_gain
-    ).astype(jnp.bfloat16)
-
     flat_ids = route_ids.reshape(-1)
+    count = flat_ids.shape[0]
     same = flat_ids[:, None] == flat_ids[None, :]
-    count = flat_ids.shape[0]
     before = jnp.arange(count)[None, :] < jnp.arange(count)[:, None]
     rank = jnp.sum((same & before).astype(jnp.int32), axis=1)
-    slot_of = ((flat_ids // 4) * 2 + rank) * 4 + flat_ids % 4
-    pair_slots = slot_of.reshape(share, top_count)
-    places = jnp.arange(device_count, dtype=jnp.int32)
-    table = jnp.zeros((device_count, share), jnp.bool_)
-    for k in range(top_count):
-        table = table | (places[:, None] == pair_slots[None, :, k])
-    outgoing = jnp.dot(table.astype(jnp.bfloat16), normed, preferred_element_type=jnp.float32)
-    outgoing = outgoing.astype(jnp.bfloat16)
-    arrived = lax.all_to_all(outgoing, ("sp", "tp"), 0, 0, tiled=True)
-    gate = jnp.einsum("sd,rdf->rsf", arrived, wg, preferred_element_type=jnp.float32)
-    upper = jnp.einsum("sd,rdf->rsf", arrived, wu, preferred_element_type=jnp.float32)
-    middle = (jax.nn.silu(gate) * upper).astype(jnp.bfloat16)
-    parts = jnp.einsum("rsf,rfd->rsd", middle, wd, preferred_element_type=jnp.float32)
-    answered = jnp.sum(parts.astype(jnp.bfloat16).astype(jnp.float32), axis=0).astype(jnp.bfloat16)
-    returned = lax.all_to_all(answered, ("sp", "tp"), 0, 0, tiled=True)
-    picked = returned[slot_of].astype(jnp.float32).reshape(share, top_count, width)
+    slots = ((flat_ids // 4) * 2 + rank) * 4 + flat_ids % 4
     route_weight = jax.nn.softmax(route_logits, axis=-1) * group_prob[:, None]
-    moe = jnp.sum(picked * route_weight[..., None], axis=1)
-    return (hidden_f + moe).astype(jnp.bfloat16)
+    out = run_experts(
+        heads, residual_in, out_weight.reshape(4, -1, width), norm_gain.reshape(1, width),
+        slots.reshape(share, -1).T, slots, route_weight.reshape(-1), wg, wu, wd,
+    )
+    return out.reshape(share, width)
 
 
 def solution(mesh):

time: 240 us -> 163 us (0.68)
  blocking collectives: 40 us -> 0 us
  Pallas kernels: 125 us -> 157 us
  waiting for transfers between devices: 30.5 us -> 0 us
  matrix products: 17.4 us -> 0 us
  local copies, waits for them, and re-layouts: 14.1 us -> 5.99 us
  starting transfers between devices: 6.63 us -> 0 us
  other arithmetic: 6.12 us -> 0.27 us
    pallas_call x0 -> x1, Pallas kernels: none -> 65.7 us  [run_experts(): pl.pallas_call(expert_kernel, out_shape=jax.ShapeDtypeStruct((share,) + t...]
    all_to_all x1 -> x0, blocking collectives: 40 us -> none  [on_device(): arrived = lax.all_to_all(outgoing, ('sp', 'tp'), 0, 0, tiled=True)]
    pallas_call x1, Pallas kernels: 125 us -> 91.1 us  [attend(): pl.pallas_call(attend_kernel, out_shape=[jax.ShapeDtypeStruct(s, bf16) fo...]
    all_to_all x1 -> x0, waiting for transfers between devices: 30.5 us -> none  [on_device(): returned = lax.all_to_all(answered, ('sp', 'tp'), 0, 0, tiled=True)]
    dot_general x4 -> x0, matrix products: 17.4 us -> none  [the longest x1 8.35 us: on_device(): jnp.einsum('rsf,rfd->rsd', middle, wd, preferred_element_type=jnp.float32)]
    all_to_all x1 -> x0, starting transfers between devices: 6.63 us -> none  [on_device(): returned = lax.all_to_all(answered, ('sp', 'tp'), 0, 0, tiled=True)]
    unnamed x20 -> x16, local copies, waits for them, and re-layouts: 8.89 us -> 3.97 us
    all_to_all x2 -> x0, other arithmetic: 2.84 us -> none  [the longest x1 1.42 us: on_device(): returned = lax.all_to_all(answered, ('sp', 'tp'), 0, 0, tiled=True)]
  transfers between devices with their start and end apart: 1 -> 0, of which waited for: 1 -> 0; matrix products, arithmetic and copies ran while one was open for 0% -> 0% of each run, Pallas kernels for 0% -> 0%
where the time goes in v2:
time: 163 us
  Pallas kernels  157 us (96%)
  local copies, waits for them, and re-layouts  5.99 us (4%)
    pallas_call x1, Pallas kernels, attend(): pl.pallas_call(attend_kernel, out_shape=[jax.ShapeDtypeStruct(s, bf16) fo...  91.1 us
    pallas_call x1, Pallas kernels, run_experts(): pl.pallas_call(expert_kernel, out_shape=jax.ShapeDtypeStruct((share,) + t...  65.7 us
    unnamed x16, local copies, waits for them, and re-layouts  3.97 us

profile of v2, /device:TPU:1, one launch (start us, length us, event | category | flops | bytes accessed | tf_op | source)
XLA Modules:
  0.0 163.1 jit_solution(14848820772635337041)
XLA Ops:
  0.0 0.0 copy-start.5
  0.0 0.0 copy-start.4
  0.0 0.0 copy-start.6
  0.0 0.0 copy-start.3
  0.0 0.0 copy-start.1
  0.0 1.4 copy.25.gain_ref
  1.5 91.1 %gather_attend.1 = (bf16[4,64,256]{2,1,0:T(8,128)(2,1)}, bf16[4,2048,256]{2,1,0:T(8,128)(2,1)}, bf16[4,2048,256]{2,1,0:T(8,128)(2,1)}, bf16[4,256,2048]{2,1,0:T(...) custom-call(bf16[256,128]{1,0:T(8,128)(2,1)} %q1_ref.1, ...), custom_call_target="tpu_custom_call" | custom-call | tf_op jit(solution)/shard_map/gather_attend/pallas_call | solution.py:419
  92.5 0.0 copy-done.5
  92.6 0.1 copy.26
  92.6 0.1 eq.17
  92.8 0.2 convert_reduce_fusion
  93.0 0.1 reduce_sum.21
  93.1 0.1 copy.27
  93.2 0.0 copy-done.4
  93.3 0.0 copy-done.6
  93.3 0.1 copy.28
  93.4 0.1 reshape.26.weight_ref
  93.5 0.0 copy-done.3
  93.6 0.0 copy-done.1
  93.6 0.0 copy-start
  93.6 2.2 %copy-done = bf16[1024,2048]{1,0:T(8,128)(2,1)S(1)} copy-done((bf16[1024,2048]{1,0:T(8,128)(2,1)S(1)}, bf16[1024,2048]{1,0:T(8,128)(2,1)}, u32[]{:S(2)}) %copy-start) | copy-done | bytes 4194328
  95.8 0.0 copy-start.2
  95.8 0.9 copy-done.2
  96.7 65.7 %experts.1 = bf16[64,16,128]{2,1,0:T(8,128)(2,1)S(1)} custom-call(bf16[4,64,256]{2,1,0:T(8,128)(2,1)S(1)} %copy-done.2, bf16[64,2048]{1,0:T(8,128)(2,1)S(1)} %copy-done.1, bf16[4,256,2048]{2,1,0:T(8,128)(2,1)S(1)} %bitcast.9, f32[1,2048]{1,0:T(1,128)S(1)} %bitcast.11, s32[2,64]{1,0:T(2,128)S(1)} %fusion.2.pair_ref, s32[128]{0:T(128)S(1)} %fusion.4.slot_ref, ...), custom_call_target="tpu_custom_call" | custom-call | tf_op jit(solution)/shard_map/experts/pallas_call | solution.py:578
  162.3 0.8 copy.31
  (5 shorter events, 0.1 us)
Async XLA Ops:
  0.0 92.5 %copy-start.5 = (s32[64,2]{0,1:T(2,128)S(1)}, s32[64,2]{0,1:T(2,128)}, u32[]{:S(2)}) copy-start(s32[64,2]{0,1:T(2,128)} %param.26) | copy-start | bytes 1540
  0.0 93.2 %copy-start.4 = (f32[64,2]{0,1:T(2,128)S(1)}, f32[64,2]{0,1:T(2,128)}, u32[]{:S(2)}) copy-start(f32[64,2]{0,1:T(2,128)} %param.27) | copy-start | bytes 1540
  0.0 93.3 %copy-start.6 = (f32[64]{0:T(128)S(1)}, f32[64]{0:T(128)}, u32[]{:S(2)}) copy-start(f32[64]{0:T(128)} %param.28) | copy-start | bytes 772
  0.0 93.5 %copy-start.3 = (f32[2048]{0:T(1024)S(1)}, f32[2048]{0:T(1024)}, u32[]{:S(2)}) copy-start(f32[2048]{0:T(1024)} %param.25) | copy-start | bytes 24580
  0.0 93.5 %copy-start.1 = (bf16[64,2048]{1,0:T(8,128)(2,1)S(1)}, bf16[64,2048]{1,0:T(8,128)(2,1)}, u32[]{:S(2)}) copy-start(bf16[64,2048]{1,0:T(8,128)(2,1)} %resid_ref.1) | copy-start | bytes 786436
  93.6 2.2 %copy-start = (bf16[1024,2048]{1,0:T(8,128)(2,1)S(1)}, bf16[1024,2048]{1,0:T(8,128)(2,1)}, u32[]{:S(2)}) copy-start(bf16[1024,2048]{1,0:T(8,128)(2,1)} %param.24) | copy-start | bytes 12582916
  95.8 0.9 copy-start.2
